TPU v7x, 32 devices: a whole 2x2x4 slice. The times are simulated.
32 devices in a mesh: fs: 8 (over z, y), tp: 4 (over x, core).
Axes of the slice: x: 2, y: 2, z: 4, core: 2. Of those that a mesh axis runs over, the one named last changes fastest.
Arguments:
- hidden_in: bfloat16 [2048, 2048], P('fs'), may hold values from -6 to 6
- mix_gain: float32 [2048], replicated, may hold values from 0.1 to 1.9
- value_proj: float32 [2048, 512], P('fs', 'tp'), may hold values from -0.125 to 0.125
- gate_proj: float32 [2048, 512], P('fs', 'tp'), may hold values from -0.125 to 0.125
- out_proj: float32 [2048, 512], P('fs', 'tp'), may hold values from -0.25 to 0.25
- value_scale: float32 [512], P('tp'), may hold values from 0.3 to 3
- gate_scale: float32 [512], P('tp'), may hold values from 0.5 to 2
- out_scale: float32 [2048], P('fs'), may hold values from 0.5 to 2
- conv_kernel: bfloat16 [31, 512], P(None, 'tp'), may hold values from -1 to 1
- norm_gain: float32 [512], P('tp'), may hold values from 0.1 to 1.9
- norm_shift: float32 [512], P('tp'), may hold values from -3 to 3
- mlp_gain: float32 [2048], replicated, may hold values from 0.1 to 1.9
- mlp_gate: float32 [2048, 2816], P('fs', 'tp'), may hold values from -0.125 to 0.125
- mlp_up: float32 [2048, 2816], P('fs', 'tp'), may hold values from -0.125 to 0.125
- mlp_down: float32 [2048, 2816], P('fs', 'tp'), may hold values from -0.109375 to 0.109375
- mlp_gate_scale: float32 [2816], P('tp'), may hold values from 0.5 to 2
- mlp_up_scale: float32 [2816], P('tp'), may hold values from 0.5 to 2
- mlp_down_scale: float32 [2048], P('fs'), may hold values from 0.5 to 2
Outputs:
- layer_out: bfloat16 [2048, 2048], P('fs')
All inputs are finite; a program needn't handle non-finite values.
Results may differ from a plain program's by a relative error of at most 0.019.
Values may be sent and summed in bfloat16 or wider, within the bound.
A program may use at most 64 MiB of HBM per device.

v0:
```python
import jax
import jax.numpy as jnp
from jax import lax
from jax.sharding import PartitionSpec as P


def row_norm(rows, gain):
    scale = lax.rsqrt(jnp.mean(rows * rows, axis=-1, keepdims=True) + 1e-06)
    return rows * scale * gain


def contract_last(left, right):
    return lax.dot_general(
        left, right, (((1,), (1,)), ((), ())), preferred_element_type=jnp.float32
    )


def body(
    hidden_in,
    mix_gain,
    value_proj,
    gate_proj,
    out_proj,
    value_scale,
    gate_scale,
    out_scale,
    conv_kernel,
    norm_gain,
    norm_shift,
    mlp_gain,
    mlp_gate,
    mlp_up,
    mlp_down,
    mlp_gate_scale,
    mlp_up_scale,
    mlp_down_scale,
):
    out_full, down_full = (
        lax.all_gather(out_scale, "fs", axis=0, tiled=True),
        lax.all_gather(mlp_down_scale, "fs", axis=0, tiled=True),
    )
    value_w, gate_w, out_w = (
        lax.all_gather(value_proj.astype(jnp.bfloat16), "fs", axis=0, tiled=True),
        lax.all_gather(gate_proj.astype(jnp.bfloat16), "fs", axis=0, tiled=True),
        lax.all_gather(out_proj.astype(jnp.bfloat16), "fs", axis=0, tiled=True),
    )
    mlp_shards = (
        mlp_gate.astype(jnp.bfloat16),
        mlp_up.astype(jnp.bfloat16),
        mlp_down.astype(jnp.bfloat16),
    )
    rows = hidden_in.astype(jnp.float32)
    normed = row_norm(rows, mix_gain).astype(jnp.bfloat16)
    value_pre = jnp.dot(normed, value_w, preferred_element_type=jnp.float32) * value_scale
    gate_pre = jnp.dot(normed, gate_w, preferred_element_type=jnp.float32) * gate_scale
    glu = value_pre * jax.nn.sigmoid(gate_pre)
    seq_len = glu.shape[0]
    taps = conv_kernel.shape[0]
    padded = jnp.pad(glu, ((taps - 1, 0), (0, 0)))
    kernel = conv_kernel.astype(jnp.float32)
    conved = jnp.zeros_like(glu)
    for tap in range(taps):
        conved = conved + padded[tap : tap + seq_len] * kernel[tap]
    channels = conved.shape[1] * lax.axis_size("tp")
    sums, squares = lax.psum((jnp.sum(conved, axis=1), jnp.sum(conved * conved, axis=1)), "tp")
    chan_mean = (sums / channels)[:, None]
    chan_var = (squares / channels)[:, None] - chan_mean * chan_mean
    act = jax.nn.silu(
        (conved - chan_mean) * lax.rsqrt(chan_var + 1e-05) * norm_gain + norm_shift
    ).astype(jnp.bfloat16)
    conv_term = contract_last(act, out_w) * out_full
    middle_f = (
        (rows + lax.psum(conv_term.astype(jnp.bfloat16), "tp").astype(jnp.float32))
        .astype(jnp.bfloat16)
        .astype(jnp.float32)
    )
    normed_mlp = row_norm(middle_f, mlp_gain).astype(jnp.bfloat16)
    collected = (
        lax.all_gather(mlp_shards[0], "fs", axis=0, tiled=True),
        lax.all_gather(mlp_shards[1], "fs", axis=0, tiled=True),
        lax.all_gather(mlp_shards[2], "fs", axis=0, tiled=True),
    )
    gate_mlp = (
        jnp.dot(normed_mlp, collected[0], preferred_element_type=jnp.float32) * mlp_gate_scale
    )
    up_mlp = jnp.dot(normed_mlp, collected[1], preferred_element_type=jnp.float32) * mlp_up_scale
    hidden_act = (jax.nn.silu(gate_mlp) * up_mlp).astype(jnp.bfloat16)
    mlp_term = contract_last(hidden_act, collected[2]) * down_full
    return (middle_f + lax.psum(mlp_term.astype(jnp.bfloat16), "tp").astype(jnp.float32)).astype(
        jnp.bfloat16
    )


def solution(mesh):
    return jax.shard_map(
        body,
        mesh=mesh,
        in_specs=(
            P("fs", None),
            P(),
            P("fs", "tp"),
            P("fs", "tp"),
            P("fs", "tp"),
            P("tp"),
            P("tp"),
            P("fs"),
            P(None, "tp"),
            P("tp"),
            P("tp"),
            P(),
            P("fs", "tp"),
            P("fs", "tp"),
            P("fs", "tp"),
            P("tp"),
            P("tp"),
            P("fs"),
        ),
        out_specs=P("fs", None),
        check_vma=False,
    )
```

profile of v0, /device:TPU:0, one launch (start us, length us, event | category | flops | bytes accessed | tf_op | source)
XLA Modules:
  0.0 370.3 jit_solution(7887861853661166801)
XLA Ops:
  7.4 0.0 all-reduce.5.cloned.1.call-start
  7.4 0.8 convert_element_type.63
  8.2 1.5 fusion.2
  9.8 0.9 convert_element_type.61
  10.7 33.0 %all_gather.24 = bf16[2048,128]{1,0:T(8,128)(2,1)S(1)} all-gather(bf16[256,128]{1,0:T(8,128)(2,1)S(1)} %convert_element_type.61), channel_id=1, replica_groups=mesh['fs'=8,'tp'=4] {'fs'}, dimensions={0}, use_global_device_ids=true | all-gather | bytes 589824 | tf_op jit(solution)/shard_map/all_gather | solution.py:43
  43.7 0.9 convert_element_type.62
  44.6 31.4 %all_gather.25 = bf16[2048,128]{1,0:T(8,128)(2,1)S(1)} all-gather(bf16[256,128]{1,0:T(8,128)(2,1)S(1)} %convert_element_type.62), channel_id=1, replica_groups=mesh['fs'=8,'tp'=4] {'fs'}, dimensions={0}, use_global_device_ids=true | all-gather | bytes 589824 | tf_op jit(solution)/shard_map/all_gather | solution.py:44
  76.0 31.3 %all_gather.26 = bf16[2048,128]{1,0:T(8,128)(2,1)S(1)} all-gather(bf16[256,128]{1,0:T(8,128)(2,1)S(1)} %convert_element_type.65), channel_id=1, replica_groups=mesh['fs'=8,'tp'=4] {'fs'}, dimensions={0}, use_global_device_ids=true | all-gather | bytes 589824 | tf_op jit(solution)/shard_map/all_gather | solution.py:45
  107.3 20.7 %all-gather = f32[8,1,256]{2,1,0:T(1,128)S(1)} all-gather(f32[1,1,256]{2,1,0:T(1,128)S(1)} %bitcast.74), channel_id=1, replica_groups=mesh['fs'=8,'tp'=4] {'fs'}, dimensions={0}, use_global_device_ids=true | all-gather | bytes 9216 | tf_op jit(solution)/shard_map/all_gather | solution.py:39
  128.1 0.5 convolution_multiply_fusion.5
  128.6 0.5 fusion.16
  129.2 0.6 fusion.91
  129.7 5.7 %all-reduce.1 = (f32[256]{0:T(256)S(1)}, f32[256]{0:T(256)S(1)}) all-reduce(f32[256]{0:T(256)S(1)} %get-tuple-element.6, f32[256]{0:T(256)S(1)} %get-tuple-element.5), channel_id=1, replica_groups=mesh['fs'=8,'tp'=4] {'tp'}, use_global_device_ids=true, to_apply=%region_4.5 | all-reduce | flops 512 | bytes 4096 | tf_op jit(solution)/shard_map/psum | solution.py:65
  135.4 1.5 fusion.1
  136.9 0.0 all-gather.6.cloned.1.call-start
  137.0 0.8 convert_element_type.71
  137.8 0.0 all-gather.10.cloned.1.call-start
  137.9 0.8 convert_element_type.74
  138.7 0.0 all-gather.8.cloned.1.call-start
  138.8 0.8 convert_element_type.72
  139.6 0.0 all-gather.8.cloned.1.call-update
  139.6 0.0 all-reduce.7.cloned.1.call-start
  139.6 16.5 %all-gather.1 = f32[8,1,256]{2,1,0:T(1,128)S(1)} all-gather(f32[1,1,256]{2,1,0:T(1,128)S(1)} %bitcast.75), channel_id=1, replica_groups=mesh['fs'=8,'tp'=4] {'fs'}, dimensions={0}, use_global_device_ids=true | all-gather | bytes 9216 | tf_op jit(solution)/shard_map/all_gather | solution.py:40
  156.2 14.7 %all-reduce.5.cloned.1.call-done = bf16[256,2048]{1,0:T(8,128)(2,1)} async-done(((bf16[256,2048]{1,0:T(8,128)(2,1)}), bf16[256,2048]{1,0:T(8,128)(2,1)}) %all-reduce.5.cloned.1.call-update) | async-done | bytes 1048592 | tf_op jit(solution)/shard_map/psum | solution.py:73
  170.9 1.8 fusion.6
  172.6 24.8 %all-gather.6.cloned.1.call-done = bf16[2048,704]{0,1:T(8,128)(2,1)} async-done(((bf16[256,704]{0,1:T(8,128)(2,1)}), bf16[2048,704]{0,1:T(8,128)(2,1)}) %all-gather.6.cloned.1.call-update) | async-done | bytes 2883600 | tf_op jit(solution)/shard_map/all_gather | solution.py:79
  197.4 2.8 convolution_multiply_fusion.3
  200.3 57.6 %all-gather.10.cloned.1.call-done = bf16[2048,704]{0,1:T(8,128)(2,1)} async-done(((bf16[256,704]{0,1:T(8,128)(2,1)}), bf16[2048,704]{0,1:T(8,128)(2,1)}) %all-gather.10.cloned.1.call-update) | async-done | bytes 2883600 | tf_op jit(solution)/shard_map/all_gather | solution.py:81
  257.9 60.5 %all-gather.8.cloned.1.call-done = bf16[2048,704]{0,1:T(8,128)(2,1)} async-done(((bf16[256,704]{0,1:T(8,128)(2,1)}), bf16[2048,704]{0,1:T(8,128)(2,1)}) %all-gather.8.cloned.1.call-update) | async-done | bytes 2883600 | tf_op jit(solution)/shard_map/all_gather | solution.py:80
  318.5 7.0 %fusion = bf16[256,2048]{1,0:T(8,128)(2,1)} fusion(bf16[2048,704]{0,1:T(8,128)(2,1)} %all-gather.10.cloned.1.call-done, f32[2048]{0:T(1024)S(1)} %bitcast.73, bf16[2048,704]{0,1:T(8,128)(2,1)} %all-gather.8.cloned.1.call-done, f32[256,704]{0,1:T(8,128)S(1)} %convolution_multiply_fusion.3, f32[704]{0:T(1024)S(1)} %copy-done.10, ...), kind=kOutput, calls=%fused_computation.8 | convolution fusion | flops 1480802304 | bytes 8605440 | tf_op jit(solution)/shard_map/dot_general | solution.py:13
  325.5 34.6 %all-reduce.7.cloned.1.call-done = bf16[256,2048]{1,0:T(8,128)(2,1)} async-done(((bf16[256,2048]{1,0:T(8,128)(2,1)}), bf16[256,2048]{1,0:T(8,128)(2,1)}) %all-reduce.7.cloned.1.call-update) | async-done | bytes 1048592 | tf_op jit(solution)/shard_map/psum | solution.py:89
  360.1 2.6 fusion.9
  (40 shorter events, 0.2 us)
Async XLA Ops:
  7.4 120.7 %copy-start = (bf16[256,2048]{1,0:T(8,128)(2,1)S(1)}, bf16[256,2048]{1,0:T(8,128)(2,1)}, u32[]{:S(2)}) copy-start(bf16[256,2048]{1,0:T(8,128)(2,1)} %param.18) | copy-start | bytes 3145732
  7.4 68.6 %copy-start.4 = (f32[256,128]{1,0:T(8,128)S(1)}, f32[256,128]{1,0:T(8,128)}, u32[]{:S(2)}) copy-start(f32[256,128]{1,0:T(8,128)} %param.22) | copy-start | bytes 393220
  7.4 100.0 %copy-start.5 = (f32[256]{0:T(256)S(1)}, f32[256]{0:T(256)}, u32[]{:S(2)}) copy-start(f32[256]{0:T(256)} %param.25) | copy-start | bytes 3076
  7.4 120.7 %copy-start.7 = (f32[2048]{0:T(1024)S(1)}, f32[2048]{0:T(1024)}, u32[]{:S(2)}) copy-start(f32[2048]{0:T(1024)} %param.19) | copy-start | bytes 24580
  7.4 120.7 %copy-start.11 = (f32[128]{0:T(128)S(1)}, f32[128]{0:T(128)}, u32[]{:S(2)}) copy-start(f32[128]{0:T(128)} %param.23) | copy-start | bytes 1540
  7.4 163.5 %all-reduce.5.cloned.1.call-start = ((), (), s32[]{:S(2)}) async-start(), calls=%async_computation | async-start | bytes 2097152 | tf_op jit(solution)/shard_map/psum | solution.py:73
  43.7 84.9 %copy-start.12 = (f32[128]{0:T(128)S(1)}, f32[128]{0:T(128)}, u32[]{:S(2)}) copy-start(f32[128]{0:T(128)} %param.24) | copy-start | bytes 1540
  128.6 6.8 %copy-start.13 = (f32[128]{0:T(128)S(1)}, f32[128]{0:T(128)}, u32[]{:S(2)}) copy-start(f32[128]{0:T(128)} %param.28) | copy-start | bytes 1540
  128.6 6.8 %copy-start.14 = (f32[128]{0:T(128)S(1)}, f32[128]{0:T(128)}, u32[]{:S(2)}) copy-start(f32[128]{0:T(128)} %param.27) | copy-start | bytes 1540
  129.1 7.9 %copy-start.1 = (f32[256,704]{0,1:T(8,128)S(1)}, f32[256,704]{0,1:T(8,128)}, u32[]{:S(2)}) copy-start(f32[256,704]{0,1:T(8,128)} %param.30) | copy-start | bytes 2162692
  135.4 2.5 copy-start.2
  136.9 1.8 copy-start.3
  136.9 2.7 copy-start.6
  136.9 60.5 %all-gather.6.cloned.1.call-start = ((), (), s32[]{:S(2)}) async-start(), calls=%async_computation.1 | async-start | bytes 3244032 | tf_op jit(solution)/shard_map/all_gather | solution.py:79
  137.8 120.1 %all-gather.10.cloned.1.call-start = ((), (), s32[]{:S(2)}) async-start(), calls=%async_computation.3 | async-start | bytes 3244032 | tf_op jit(solution)/shard_map/all_gather | solution.py:81
  138.7 58.8 %copy-start.8 = (f32[2048]{0:T(1024)S(1)}, f32[2048]{0:T(1024)}, u32[]{:S(2)}) copy-start(f32[2048]{0:T(1024)} %param.29) | copy-start | bytes 24580
  138.7 58.8 %copy-start.9 = (f32[704]{0:T(1024)S(1)}, f32[704]{0:T(1024)}, u32[]{:S(2)}) copy-start(f32[704]{0:T(1024)} %param.33) | copy-start | bytes 8452
  138.7 179.8 %all-gather.8.cloned.1.call-start = ((), (), s32[]{:S(2)}) async-start(), calls=%async_computation.2 | async-start | bytes 3244032 | tf_op jit(solution)/shard_map/all_gather | solution.py:80
  139.6 220.6 %all-reduce.7.cloned.1.call-start = ((), (), s32[]{:S(2)}) async-start(), calls=%async_computation.4 | async-start | bytes 2097152 | tf_op jit(solution)/shard_map/psum | solution.py:89
  197.4 121.0 %copy-start.10 = (f32[704]{0:T(1024)S(1)}, f32[704]{0:T(1024)}, u32[]{:S(2)}) copy-start(f32[704]{0:T(1024)} %param.34) | copy-start | bytes 8452
Sparse Core Ops, SparseCore 0:
  137.1 33.7 all-reduce.4
  325.6 34.4 all-reduce.6
Sparse Core Ops, SparseCore 1:
  139.5 57.9 all-gather.5
  199.3 58.5 all-gather.9
  259.9 58.5 all-gather.7
where the time goes:
time: 371 us; the launch traced here: 370 us
  waiting for transfers between devices  192 us (52%)
  blocking collectives  139 us (37%)
  between operations  15.2 us (4%)
  matrix products  12.4 us (3%)
  other arithmetic  11.4 us (3%)
    all_gather x1, waiting for transfers between devices, body(): lax.all_gather(mlp_shards[1], 'fs', axis=0, tiled=True)  60.5 us
    all_gather x1, waiting for transfers between devices, body(): lax.all_gather(mlp_shards[2], 'fs', axis=0, tiled=True)  57.6 us
    psum x1, waiting for transfers between devices, body(): lax.psum(mlp_term.astype(jnp.bfloat16), 'tp').astype(jnp.float32)  34.6 us
    all_gather x1, blocking collectives, body(): lax.all_gather(value_proj.astype(jnp.bfloat16), 'fs', axis=0, tiled=True)  33 us
    all_gather x1, blocking collectives, body(): lax.all_gather(gate_proj.astype(jnp.bfloat16), 'fs', axis=0, tiled=True)  31.4 us
    all_gather x1, blocking collectives, body(): lax.all_gather(out_proj.astype(jnp.bfloat16), 'fs', axis=0, tiled=True)  31.3 us
    all_gather x1, waiting for transfers between devices, body(): lax.all_gather(mlp_shards[0], 'fs', axis=0, tiled=True)  24.8 us
    all_gather x1, blocking collectives, body(): lax.all_gather(out_scale, 'fs', axis=0, tiled=True)  20.7 us
  transfers between devices with their start and end apart: 5, of which 5 were waited for; matrix products, arithmetic and copies ran while one was open for 2% of the time, Pallas kernels for 0%

commit v1 on v0

--- a/solution.py
+++ b/solution.py
@@ -2,6 +2,24 @@
 import jax.numpy as jnp
 from jax import lax
 from jax.sharding import PartitionSpec as P
+
+
+def gather_around(array, axis, dim):
+    ways, here, step = (lax.axis_size(axis), lax.axis_index(axis), array.shape[dim])
+    shape = [n * ways if d == dim else n for d, n in enumerate(array.shape)]
+    full = lax.dynamic_update_slice_in_dim(
+        jnp.zeros(shape, array.dtype), array, here * step, axis=dim
+    )
+    going_up = going_down = array
+    for far in range(1, ways // 2 + 1):
+        going_up = lax.ppermute(going_up, axis, [(d, (d + 1) % ways) for d in range(ways)])
+        full = lax.dynamic_update_slice_in_dim(full, going_up, (here - far) % ways * step, axis=dim)
+        if 2 * far < ways:
+            going_down = lax.ppermute(going_down, axis, [(d, (d - 1) % ways) for d in range(ways)])
+            full = lax.dynamic_update_slice_in_dim(
+                full, going_down, (here + far) % ways * step, axis=dim
+            )
+    return full
 
 
 def row_norm(rows, gain):
@@ -77,7 +95,7 @@
     normed_mlp = row_norm(middle_f, mlp_gain).astype(jnp.bfloat16)
     collected = (
         lax.all_gather(mlp_shards[0], "fs", axis=0, tiled=True),
-        lax.all_gather(mlp_shards[1], "fs", axis=0, tiled=True),
+        gather_around(mlp_shards[1], "fs", 0),
         lax.all_gather(mlp_shards[2], "fs", axis=0, tiled=True),
     )
     gate_mlp = (

time: 371 us -> 349 us (0.941)
  waiting for transfers between devices: 192 us -> 139 us
  starting transfers between devices: 0.21 us -> 14.4 us
  blocking collectives: 139 us -> 148 us
  local copies, waits for them, and re-layouts: 0.09 us -> 7.63 us
    all_gather x1 -> x0, waiting for transfers between devices: 60.5 us -> none  [body(): lax.all_gather(mlp_shards[1], 'fs', axis=0, tiled=True)]
    ppermute x0 -> x7, waiting for transfers between devices: none -> 45.2 us  [the longest x3 26.2 us: gather_around(): lax.ppermute(going_down, axis, [(d, (d - 1) % ways) for d in range(ways)])]
    all_gather x1, waiting for transfers between devices: 24.8 us -> 0.01 us  [body(): lax.all_gather(mlp_shards[0], 'fs', axis=0, tiled=True)]
    psum x1, waiting for transfers between devices: 14.7 us -> 0.01 us  [body(): lax.psum(conv_term.astype(jnp.bfloat16), 'tp').astype(jnp.float32)]
    ppermute x0 -> x7, starting transfers between devices: none -> 14.2 us  [the longest x4 7.14 us: gather_around(): lax.ppermute(going_up, axis, [(d, (d + 1) % ways) for d in range(ways)])]
    all_gather x1, blocking collectives: 16.5 us -> 25.7 us  [body(): lax.all_gather(mlp_down_scale, 'fs', axis=0, tiled=True)]
    dynamic_update_slice x0 -> x7, local copies, waits for them, and re-layouts: none -> 5.56 us  [the longest x4 3.18 us: gather_around(): lax.dynamic_update_slice_in_dim(full, going_up, (here - far) % ways * ste...]
  transfers between devices with their start and end apart: 5 -> 11, of which waited for: 5 -> 6; matrix products, arithmetic and copies ran while one was open for 2% -> 4% of each run, Pallas kernels for 0% -> 0%
where the time goes in v1:
time: 349 us
  blocking collectives  148 us (42%)
  waiting for transfers between devices  139 us (40%)
  between operations  15 us (4%)
  starting transfers between devices  14.4 us (4%)
  matrix products  12.5 us (4%)
  other arithmetic  12.4 us (4%)
  local copies, waits for them, and re-layouts  7.63 us (2%)
    all_gather x1, waiting for transfers between devices, body(): lax.all_gather(mlp_shards[2], 'fs', axis=0, tiled=True)  59.5 us
    psum x1, waiting for transfers between devices, body(): lax.psum(mlp_term.astype(jnp.bfloat16), 'tp').astype(jnp.float32)  34.6 us
    all_gather x1, blocking collectives, body(): lax.all_gather(value_proj.astype(jnp.bfloat16), 'fs', axis=0, tiled=True)  33 us
    all_gather x1, blocking collectives, body(): lax.all_gather(gate_proj.astype(jnp.bfloat16), 'fs', axis=0, tiled=True)  31.4 us
    all_gather x1, blocking collectives, body(): lax.all_gather(out_proj.astype(jnp.bfloat16), 'fs', axis=0, tiled=True)  31.4 us
    ppermute x3, waiting for transfers between devices, gather_around(): lax.ppermute(going_down, axis, [(d, (d - 1) % ways) for d in range(ways)])  26.2 us
    all_gather x1, blocking collectives, body(): lax.all_gather(mlp_down_scale, 'fs', axis=0, tiled=True)  25.7 us
    all_gather x1, blocking collectives, body(): lax.all_gather(out_scale, 'fs', axis=0, tiled=True)  20.6 us
  transfers between devices with their start and end apart: 11, of which 6 were waited for; matrix products, arithmetic and copies ran while one was open for 4% of the time, Pallas kernels for 0%

profile of v1, /device:TPU:0, one launch (start us, length us, event | category | flops | bytes accessed | tf_op | source)
XLA Modules:
  0.0 349.0 jit_solution(7002372015008516786)
XLA Ops:
  8.2 1.5 fusion.2
  9.8 0.9 convert_element_type.61
  10.7 33.0 %all_gather.21 = bf16[2048,128]{1,0:T(8,128)(2,1)S(1)} all-gather(bf16[256,128]{1,0:T(8,128)(2,1)S(1)} %convert_element_type.61), channel_id=1, replica_groups=mesh['fs'=8,'tp'=4] {'fs'}, dimensions={0}, use_global_device_ids=true | all-gather | bytes 589824 | tf_op jit(solution)/shard_map/all_gather | solution.py:61
  43.7 0.9 convert_element_type.62
  44.6 31.4 %all_gather.22 = bf16[2048,128]{1,0:T(8,128)(2,1)S(1)} all-gather(bf16[256,128]{1,0:T(8,128)(2,1)S(1)} %convert_element_type.62), channel_id=1, replica_groups=mesh['fs'=8,'tp'=4] {'fs'}, dimensions={0}, use_global_device_ids=true | all-gather | bytes 589824 | tf_op jit(solution)/shard_map/all_gather | solution.py:62
  76.0 0.9 convert_element_type.65
  76.9 31.4 %all_gather.23 = bf16[2048,128]{1,0:T(8,128)(2,1)S(1)} all-gather(bf16[256,128]{1,0:T(8,128)(2,1)S(1)} %convert_element_type.65), channel_id=1, replica_groups=mesh['fs'=8,'tp'=4] {'fs'}, dimensions={0}, use_global_device_ids=true | all-gather | bytes 589824 | tf_op jit(solution)/shard_map/all_gather | solution.py:63
  108.3 20.6 %all-gather = f32[8,1,256]{2,1,0:T(1,128)S(1)} all-gather(f32[1,1,256]{2,1,0:T(1,128)S(1)} %bitcast.74), channel_id=1, replica_groups=mesh['fs'=8,'tp'=4] {'fs'}, dimensions={0}, use_global_device_ids=true | all-gather | bytes 9216 | tf_op jit(solution)/shard_map/all_gather | solution.py:57
  130.5 5.7 %all-reduce.1 = (f32[256]{0:T(256)S(1)}, f32[256]{0:T(256)S(1)}) all-reduce(f32[256]{0:T(256)S(1)} %get-tuple-element.6, f32[256]{0:T(256)S(1)} %get-tuple-element.5), channel_id=1, replica_groups=mesh['fs'=8,'tp'=4] {'tp'}, use_global_device_ids=true, to_apply=%region_4.5 | all-reduce | flops 512 | bytes 4096 | tf_op jit(solution)/shard_map/psum | solution.py:83
  136.2 1.5 fusion.1
  137.8 0.8 convert_element_type.71
  139.5 2.0 broadcast_in_dim.2
  141.5 0.8 constant_dynamic-update-slice_fusion.7
  142.4 4.7 %collective-permute-start.1 = (bf16[256,704]{0,1:T(8,128)(2,1)S(1)}, bf16[256,704]{0,1:T(8,128)(2,1)S(1)}, u32[]{:S(2)}, u32[]{:S(2)}) collective-permute-start(bf16[256,704]{0,1:T(8,128)(2,1)S(1)} %get-tuple-element.12), channel_id=1, source_target_pairs={{0,28},{4,0},{8,4},{12,8},{16,12},{20,16},{24,20},{28,24},{1,29},{... | collective-permute-start | bytes 1081352 | tf_op jit(solution)/shard_map/ppermute | solution.py:18
  147.1 14.8 %collective-permute-done = bf16[256,704]{0,1:T(8,128)(2,1)S(1)} collective-permute-done((bf16[256,704]{0,1:T(8,128)(2,1)S(1)}, bf16[256,704]{0,1:T(8,128)(2,1)S(1)}, u32[]{:S(2)}, u32[]{:S(2)}) %collective-permute-start) | collective-permute-done | bytes 360480 | tf_op jit(solution)/shard_map/ppermute | solution.py:15
  161.9 2.5 collective-permute-start.2
  164.4 25.7 %all-gather.1 = f32[8,1,256]{2,1,0:T(1,128)S(1)} all-gather(f32[1,1,256]{2,1,0:T(1,128)S(1)} %bitcast.75), channel_id=1, replica_groups=mesh['fs'=8,'tp'=4] {'fs'}, dimensions={0}, use_global_device_ids=true | all-gather | bytes 9216 | tf_op jit(solution)/shard_map/all_gather | solution.py:58
  190.1 2.4 collective-permute-start.3
  192.5 0.8 constant_dynamic-update-slice_fusion.6
  194.1 1.7 fusion.6
  195.9 20.0 %collective-permute-done.3 = bf16[256,704]{0,1:T(8,128)(2,1)S(1)} collective-permute-done((bf16[256,704]{0,1:T(8,128)(2,1)S(1)}, bf16[256,704]{0,1:T(8,128)(2,1)S(1)}, u32[]{:S(2)}, u32[]{:S(2)}) %collective-permute-start.3) | collective-permute-done | bytes 360480 | tf_op jit(solution)/shard_map/ppermute | solution.py:18
  215.9 0.8 constant_dynamic-update-slice_fusion.4
  216.7 4.6 %collective-permute-start.6 = (bf16[256,704]{0,1:T(8,128)(2,1)S(1)}, bf16[256,704]{0,1:T(8,128)(2,1)S(1)}, u32[]{:S(2)}, u32[]{:S(2)}) collective-permute-start(bf16[256,704]{0,1:T(8,128)(2,1)S(1)} %collective-permute-done.4), channel_id=1, source_target_pairs={{0,4},{4,8},{8,12},{12,16},{16,20},{20,24},{24,28},{28,0},{1,5},{5... | collective-permute-start | bytes 1081352 | tf_op jit(solution)/shard_map/ppermute | solution.py:15
  222.8 6.2 %collective-permute-done.5 = bf16[256,704]{0,1:T(8,128)(2,1)S(1)} collective-permute-done((bf16[256,704]{0,1:T(8,128)(2,1)S(1)}, bf16[256,704]{0,1:T(8,128)(2,1)S(1)}, u32[]{:S(2)}, u32[]{:S(2)}) %collective-permute-start.5) | collective-permute-done | bytes 360480 | tf_op jit(solution)/shard_map/ppermute | solution.py:18
  229.0 0.8 constant_dynamic-update-slice_fusion.1
  229.9 4.2 %collective-permute-done.6 = bf16[256,704]{0,1:T(8,128)(2,1)S(1)} collective-permute-done((bf16[256,704]{0,1:T(8,128)(2,1)S(1)}, bf16[256,704]{0,1:T(8,128)(2,1)S(1)}, u32[]{:S(2)}, u32[]{:S(2)}) %collective-permute-start.6) | collective-permute-done | bytes 360480 | tf_op jit(solution)/shard_map/ppermute | solution.py:15
  234.1 0.8 constant_dynamic-update-slice_fusion
  234.9 2.9 convolution_multiply_fusion.3
  237.8 59.5 %all-gather.7.cloned.1.call-done = bf16[2048,704]{0,1:T(8,128)(2,1)} async-done(((bf16[256,704]{0,1:T(8,128)(2,1)}), bf16[2048,704]{0,1:T(8,128)(2,1)}) %all-gather.7.cloned.1.call-update) | async-done | bytes 2883600 | tf_op jit(solution)/shard_map/all_gather | solution.py:99
  297.3 7.0 %fusion = bf16[256,2048]{1,0:T(8,128)(2,1)} fusion(bf16[2048,704]{0,1:T(8,128)(2,1)} %all-gather.7.cloned.1.call-done, f32[2048]{0:T(1024)S(1)} %bitcast.72, bf16[2048,704]{0,1:T(8,128)(2,1)} %constant_dynamic-update-slice_fusion, f32[256,704]{0,1:T(8,128)S(1)} %convolution_multiply_fusion.3, f32[704]{0:T(1024)S(1)} %copy-done.9, ...), kind=kOutput, calls=%fused_computation.8 | convolution fusion | flops 1480802304 | bytes 8605440 | tf_op jit(solution)/shard_map/dot_general | solution.py:31
  304.4 34.6 %all-reduce.7.cloned.1.call-done = bf16[256,2048]{1,0:T(8,128)(2,1)} async-done(((bf16[256,2048]{1,0:T(8,128)(2,1)}), bf16[256,2048]{1,0:T(8,128)(2,1)}) %all-reduce.7.cloned.1.call-update) | async-done | bytes 1048592 | tf_op jit(solution)/shard_map/psum | solution.py:107
  339.0 2.6 fusion.9
  (57 shorter events, 5.9 us)
Async XLA Ops:
  7.4 121.5 %copy-start = (bf16[256,2048]{1,0:T(8,128)(2,1)S(1)}, bf16[256,2048]{1,0:T(8,128)(2,1)}, u32[]{:S(2)}) copy-start(bf16[256,2048]{1,0:T(8,128)(2,1)} %param.18) | copy-start | bytes 3145732
  7.4 100.9 %copy-start.4 = (f32[256]{0:T(256)S(1)}, f32[256]{0:T(256)}, u32[]{:S(2)}) copy-start(f32[256]{0:T(256)} %param.25) | copy-start | bytes 3076
  7.4 121.5 %copy-start.6 = (f32[2048]{0:T(1024)S(1)}, f32[2048]{0:T(1024)}, u32[]{:S(2)}) copy-start(f32[2048]{0:T(1024)} %param.19) | copy-start | bytes 24580
  7.4 121.5 %copy-start.10 = (f32[128]{0:T(128)S(1)}, f32[128]{0:T(128)}, u32[]{:S(2)}) copy-start(f32[128]{0:T(128)} %param.23) | copy-start | bytes 1540
  7.4 186.8 %all-reduce.5.cloned.1.call-start = ((), (), s32[]{:S(2)}) async-start(), calls=%async_computation | async-start | bytes 2097152 | tf_op jit(solution)/shard_map/psum | solution.py:91
  8.2 121.2 %copy-start.11 = (f32[128]{0:T(128)S(1)}, f32[128]{0:T(128)}, u32[]{:S(2)}) copy-start(f32[128]{0:T(128)} %param.24) | copy-start | bytes 1540
  128.9 7.3 %copy-start.12 = (f32[128]{0:T(128)S(1)}, f32[128]{0:T(128)}, u32[]{:S(2)}) copy-start(f32[128]{0:T(128)} %param.28) | copy-start | bytes 1540
  128.9 7.3 %copy-start.13 = (f32[128]{0:T(128)S(1)}, f32[128]{0:T(128)}, u32[]{:S(2)}) copy-start(f32[128]{0:T(128)} %param.27) | copy-start | bytes 1540
  129.4 8.4 %copy-start.1 = (f32[256,704]{0,1:T(8,128)S(1)}, f32[256,704]{0,1:T(8,128)}, u32[]{:S(2)}) copy-start(f32[256,704]{0,1:T(8,128)} %param.30) | copy-start | bytes 2162692
  130.0 8.7 %copy-start.2 = (f32[256,704]{0,1:T(8,128)S(1)}, f32[256,704]{0,1:T(8,128)}, u32[]{:S(2)}) copy-start(f32[256,704]{0,1:T(8,128)} %param.32) | copy-start | bytes 2162692
  137.7 3.8 %copy-start.3 = (f32[256,704]{0,1:T(8,128)S(1)}, f32[256,704]{0,1:T(8,128)}, u32[]{:S(2)}) copy-start(f32[256,704]{0,1:T(8,128)} %param.31) | copy-start | bytes 2162692
  137.7 97.1 %all-gather.5.cloned.1.call-start = ((), (), s32[]{:S(2)}) async-start(), calls=%async_computation.1 | async-start | bytes 3244032 | tf_op jit(solution)/shard_map/all_gather | solution.py:97
  138.6 25.8 %copy-start.5 = (f32[256]{0:T(256)S(1)}, f32[256]{0:T(256)}, u32[]{:S(2)}) copy-start(f32[256]{0:T(256)} %param.35) | copy-start | bytes 3076
  138.6 158.7 %all-gather.7.cloned.1.call-start = ((), (), s32[]{:S(2)}) async-start(), calls=%async_computation.2 | async-start | bytes 3244032 | tf_op jit(solution)/shard_map/all_gather | solution.py:99
  139.5 199.5 %all-reduce.7.cloned.1.call-start = ((), (), s32[]{:S(2)}) async-start(), calls=%async_computation.3 | async-start | bytes 2097152 | tf_op jit(solution)/shard_map/psum | solution.py:107
  142.4 19.6 %collective-permute-start = (bf16[256,704]{0,1:T(8,128)(2,1)S(1)}, bf16[256,704]{0,1:T(8,128)(2,1)S(1)}, u32[]{:S(2)}, u32[]{:S(2)}) collective-permute-start(bf16[256,704]{0,1:T(8,128)(2,1)S(1)} %get-tuple-element.12), channel_id=1, source_target_pairs={{0,4},{4,8},{8,12},{12,16},{16,20},{20,24},{24,28},{28,0},{1,5},{5... | collective-permute-start | bytes 1081352 | tf_op jit(solution)/shard_map/ppermute | solution.py:15
  142.4 47.8 %collective-permute-start.1 = (bf16[256,704]{0,1:T(8,128)(2,1)S(1)}, bf16[256,704]{0,1:T(8,128)(2,1)S(1)}, u32[]{:S(2)}, u32[]{:S(2)}) collective-permute-start(bf16[256,704]{0,1:T(8,128)(2,1)S(1)} %get-tuple-element.12), channel_id=1, source_target_pairs={{0,28},{4,0},{8,4},{12,8},{16,12},{20,16},{24,20},{28,24},{1,29},{... | collective-permute-start | bytes 1081352 | tf_op jit(solution)/shard_map/ppermute | solution.py:18
  161.9 32.2 %collective-permute-start.2 = (bf16[256,704]{0,1:T(8,128)(2,1)S(1)}, bf16[256,704]{0,1:T(8,128)(2,1)S(1)}, u32[]{:S(2)}, u32[]{:S(2)}) collective-permute-start(bf16[256,704]{0,1:T(8,128)(2,1)S(1)} %collective-permute-done), channel_id=1, source_target_pairs={{0,4},{4,8},{8,12},{12,16},{16,20},{20,24},{24,28},{28,0},{1,5},{5... | collective-permute-start | bytes 1081352 | tf_op jit(solution)/shard_map/ppermute | solution.py:15
  190.1 25.7 %collective-permute-start.3 = (bf16[256,704]{0,1:T(8,128)(2,1)S(1)}, bf16[256,704]{0,1:T(8,128)(2,1)S(1)}, u32[]{:S(2)}, u32[]{:S(2)}) collective-permute-start(bf16[256,704]{0,1:T(8,128)(2,1)S(1)} %collective-permute-done.1), channel_id=1, source_target_pairs={{0,28},{4,0},{8,4},{12,8},{16,12},{20,16},{24,20},{28,24},{1,29},{... | collective-permute-start | bytes 1081352 | tf_op jit(solution)/shard_map/ppermute | solution.py:18
  194.1 40.8 %copy-start.8 = (f32[704]{0:T(1024)S(1)}, f32[704]{0:T(1024)}, u32[]{:S(2)}) copy-start(f32[704]{0:T(1024)} %param.33) | copy-start | bytes 8452
  194.1 22.6 %collective-permute-start.4 = (bf16[256,704]{0,1:T(8,128)(2,1)S(1)}, bf16[256,704]{0,1:T(8,128)(2,1)S(1)}, u32[]{:S(2)}, u32[]{:S(2)}) collective-permute-start(bf16[256,704]{0,1:T(8,128)(2,1)S(1)} %collective-permute-done.2), channel_id=1, source_target_pairs={{0,4},{4,8},{8,12},{12,16},{16,20},{20,24},{24,28},{28,0},{1,5},{5... | collective-permute-start | bytes 1081352 | tf_op jit(solution)/shard_map/ppermute | solution.py:15
  215.9 13.2 %collective-permute-start.5 = (bf16[256,704]{0,1:T(8,128)(2,1)S(1)}, bf16[256,704]{0,1:T(8,128)(2,1)S(1)}, u32[]{:S(2)}, u32[]{:S(2)}) collective-permute-start(bf16[256,704]{0,1:T(8,128)(2,1)S(1)} %collective-permute-done.3), channel_id=1, source_target_pairs={{0,28},{4,0},{8,4},{12,8},{16,12},{20,16},{24,20},{28,24},{1,29},{... | collective-permute-start | bytes 1081352 | tf_op jit(solution)/shard_map/ppermute | solution.py:18
  216.7 17.4 %collective-permute-start.6 = (bf16[256,704]{0,1:T(8,128)(2,1)S(1)}, bf16[256,704]{0,1:T(8,128)(2,1)S(1)}, u32[]{:S(2)}, u32[]{:S(2)}) collective-permute-start(bf16[256,704]{0,1:T(8,128)(2,1)S(1)} %collective-permute-done.4), channel_id=1, source_target_pairs={{0,4},{4,8},{8,12},{12,16},{16,20},{20,24},{24,28},{28,0},{1,5},{5... | collective-permute-start | bytes 1081352 | tf_op jit(solution)/shard_map/ppermute | solution.py:15
  234.9 62.5 %copy-start.7 = (f32[2048]{0:T(1024)S(1)}, f32[2048]{0:T(1024)}, u32[]{:S(2)}) copy-start(f32[2048]{0:T(1024)} %param.29) | copy-start | bytes 24580
  234.9 62.5 %copy-start.9 = (f32[704]{0:T(1024)S(1)}, f32[704]{0:T(1024)}, u32[]{:S(2)}) copy-start(f32[704]{0:T(1024)} %param.34) | copy-start | bytes 8452
Sparse Core Ops, SparseCore 0:
  137.8 33.6 all-reduce.4
  304.5 34.4 all-reduce.6
Sparse Core Ops, SparseCore 1:
  140.3 91.8 all-gather.4
  234.0 63.3 all-gather.6
